TPU v7x, 32 devices: a whole 2x2x4 slice. The times are simulated.
32 devices in a mesh: sp: 8 (over z, y), tp: 4 (over x, core).
Axes of the slice: x: 2, y: 2, z: 4, core: 2. Of those that a mesh axis runs over, the one named last changes fastest.
Arguments:
- tokens: bfloat16 [6, 2048, 2048], P(None, 'sp', 'tp'), may hold values from -6 to 6
- norm_gains: float32 [3, 2048], replicated, may hold values from 0.5 to 1.5
- weight_outer: bfloat16 [3, 2048, 1024], P(None, 'sp', 'tp'), may hold values from -0.125 to 0.125
- weight_inner: bfloat16 [3, 2048, 1024], P(None, 'sp', 'tp'), may hold values from -0.125 to 0.125
- weight_value: bfloat16 [3, 2048, 1024], P(None, 'sp', 'tp'), may hold values from -0.125 to 0.125
- conv_taps: bfloat16 [3, 3, 1024], P(None, None, 'tp'), may hold values from -3.5 to 3.5
- weight_output: bfloat16 [3, 1024, 2048], P(None, 'sp', 'tp'), may hold values from -0.1875 to 0.1875
Outputs:
- mixed_out: float32 [6, 2048, 2048], P(None, 'sp', 'tp')
All inputs are finite; a program needn't handle non-finite values.
Results may differ from a plain program's by a relative error of at most 0.03.
Values may be sent and summed in bfloat16 or wider, within the bound.
A program may use at most 128 MiB of HBM per device.

v0:
```python
import jax
import jax.numpy as jnp
from jax import lax
from jax.sharding import PartitionSpec as P

epsilon = 1e-06


def taken_in(array, axis, dim, take_in, carry):
    whole = jax.tree.map(lambda part: lax.all_gather(part, axis, axis=dim, tiled=True), array)
    return take_in(carry, whole, jnp.int32(0))


def from_behind(block, axis, distance):
    devices = range(lax.axis_size(axis))
    route = [(i - distance, i) for i in devices if i - distance in devices]
    return lax.ppermute(block, axis, route)


def normalize(values_in, gain_row):
    values = values_in.astype(jnp.float32)
    scale = lax.rsqrt(jnp.mean(values * values, axis=-1, keepdims=True) + epsilon)
    return (values * scale * gain_row.astype(jnp.float32)).astype(jnp.bfloat16)


def convolve(extended, taps):
    width = taps.shape[0]
    out_rows = extended.shape[1] - (width - 1)
    total = jnp.zeros((extended.shape[0], out_rows, extended.shape[2]), jnp.float32)
    for offset in range(width):
        total = total + taps[offset].astype(jnp.float32) * extended[:, offset : offset + out_rows]
    return total


def project_input(normed, pieces_in):
    empty = jnp.zeros((normed.shape[0], pieces_in[0].shape[1]), jnp.float32)

    def add_rows(totals, pieces, start):
        columns = lax.dynamic_slice_in_dim(normed, start, pieces[0].shape[0], 1)
        return tuple(
            (
                total + jnp.dot(columns, piece, preferred_element_type=jnp.float32)
                for total, piece in zip(totals, pieces)
            )
        )

    return taken_in(
        (pieces_in[0], pieces_in[1], pieces_in[2]), "sp", 0, add_rows, (empty, empty, empty)
    )


def project_output(flat_mix, piece_in):
    empty = jnp.zeros((flat_mix.shape[0], piece_in.shape[1]), jnp.float32)

    def add_rows(total, piece, start):
        columns = lax.dynamic_slice_in_dim(flat_mix, start, piece.shape[0], 1)
        return total + jnp.dot(columns, piece, preferred_element_type=jnp.float32)

    return taken_in(piece_in, "sp", 0, add_rows, empty)


def local(tokens, norm_gains, weight_outer, weight_inner, weight_value, conv_taps, weight_output):
    layers = conv_taps.shape[0]
    history = conv_taps.shape[1] - 1
    sequences = tokens.shape[0]
    current = tokens
    result = None
    for layer in range(layers):
        rows = current.shape[1]
        whole = lax.all_gather(current, "tp", axis=2, tiled=True)
        normed = normalize(whole, norm_gains[layer]).reshape(sequences * rows, whole.shape[2])
        outer, inner, value = project_input(
            normed, (weight_outer[layer], weight_inner[layer], weight_value[layer])
        )
        outer = outer.astype(jnp.bfloat16)
        inner = inner.astype(jnp.bfloat16)
        value = value.astype(jnp.bfloat16)
        outer, inner, value = lax.optimization_barrier((outer, inner, value))
        channels = outer.shape[1]
        outer = outer.reshape(sequences, rows, channels)
        gated = (inner.astype(jnp.float32) * value.astype(jnp.float32)).reshape(
            sequences, rows, channels
        )
        earlier = from_behind(gated[:, rows - history :], "sp", 1)
        extended = jnp.concatenate([earlier, gated], axis=1)
        kept = outer
        conved = convolve(extended, conv_taps[layer])
        mixer = (kept.astype(jnp.float32) * conved).astype(jnp.bfloat16)
        out_rows = mixer.shape[1]
        full_mix = lax.all_gather(mixer, "tp", axis=2, tiled=True)
        flat_mix = full_mix.reshape(sequences * out_rows, full_mix.shape[2])
        projected = project_output(flat_mix, weight_output[layer])
        result = projected.reshape(sequences, out_rows, projected.shape[1])
        current = result.astype(jnp.bfloat16)
    return result


def solution(mesh):
    placed = (
        P(None, "sp", "tp"),
        P(),
        P(None, "sp", "tp"),
        P(None, "sp", "tp"),
        P(None, "sp", "tp"),
        P(None, None, "tp"),
        P(None, "sp", "tp"),
    )
    return jax.shard_map(
        local, mesh=mesh, in_specs=placed, out_specs=P(None, "sp", "tp"), check_vma=False
    )
```

profile of v0, /device:TPU:0, one launch (start us, length us, event | category | flops | bytes accessed | tf_op | source)
XLA Modules:
  0.0 757.6 jit_solution(11629076176349233693)
XLA Ops:
  8.4 0.8 fusion.45
  9.2 0.7 fusion.46
  10.0 0.8 fusion.43
  10.9 47.1 %all-gather.31.cloned.1.call-done = bf16[6,256,2048]{2,1,0:T(8,128)(2,1)} async-done(((bf16[6,256,512]{2,1,0:T(8,128)(2,1)}), bf16[6,256,2048]{2,1,0:T(8,128)(2,1)}) %all-gather.31.cloned.1.call-update) | async-done | bytes 6291472 | tf_op jit(solution)/shard_map/all_gather | solution.py:70
  58.0 4.2 fusion
  62.6 4.2 fusion.2
  66.8 33.7 %all-gather.47.cloned.1.call-done = bf16[1,2048,256]{2,1,0:T(8,128)(2,1)} async-done(((bf16[1,256,256]{2,1,0:T(8,128)(2,1)}), bf16[1,2048,256]{2,1,0:T(8,128)(2,1)}) %all-gather.47.cloned.1.call-update) | async-done | bytes 1048592 | tf_op jit(solution)/shard_map/all_gather | solution.py:10
  100.4 4.8 convolution_convert_fusion.6
  105.3 36.3 %all-gather.45.cloned.1.call-done = bf16[1,2048,256]{2,1,0:T(8,128)(2,1)} async-done(((bf16[1,256,256]{2,1,0:T(8,128)(2,1)}), bf16[1,2048,256]{2,1,0:T(8,128)(2,1)}) %all-gather.45.cloned.1.call-update) | async-done | bytes 1048592 | tf_op jit(solution)/shard_map/all_gather | solution.py:10
  141.6 4.9 convolution_convert_fusion.7
  146.5 36.1 %all-gather.43.cloned.1.call-done = bf16[1,2048,256]{2,1,0:T(8,128)(2,1)} async-done(((bf16[1,256,256]{2,1,0:T(8,128)(2,1)}), bf16[1,2048,256]{2,1,0:T(8,128)(2,1)}) %all-gather.43.cloned.1.call-update) | async-done | bytes 1048592 | tf_op jit(solution)/shard_map/all_gather | solution.py:10
  182.6 4.8 convolution_convert_fusion.8
  187.7 2.5 collective-permute-start
  190.2 1.4 collective-permute-done
  191.5 1.5 fusion.26
  193.1 30.5 %all-gather.49.cloned.1.call-done = bf16[1,1024,512]{2,1,0:T(8,128)(2,1)} async-done(((bf16[1,128,512]{2,1,0:T(8,128)(2,1)}), bf16[1,1024,512]{2,1,0:T(8,128)(2,1)}) %all-gather.49.cloned.1.call-update) | async-done | bytes 1048592 | tf_op jit(solution)/shard_map/all_gather | solution.py:10
  223.6 29.1 %all-gather.33.cloned.1.call-done = bf16[6,256,1024]{2,1,0:T(8,128)(2,1)} async-done(((bf16[6,256,256]{2,1,0:T(8,128)(2,1)}), bf16[6,256,1024]{2,1,0:T(8,128)(2,1)}) %all-gather.33.cloned.1.call-update) | async-done | bytes 3145744 | tf_op jit(solution)/shard_map/all_gather | solution.py:90
  252.7 5.1 convolution_convert_fusion.10
  260.8 43.5 %all-gather.35.cloned.1.call-done = bf16[6,256,2048]{2,1,0:T(8,128)(2,1)} async-done(((bf16[6,256,512]{2,1,0:T(8,128)(2,1)}), bf16[6,256,2048]{2,1,0:T(8,128)(2,1)}) %all-gather.35.cloned.1.call-update) | async-done | bytes 6291472 | tf_op jit(solution)/shard_map/all_gather | solution.py:70
  304.3 4.2 fusion.3
  308.9 4.2 fusion.5
  313.1 33.7 %all-gather.55.cloned.1.call-done = bf16[1,2048,256]{2,1,0:T(8,128)(2,1)} async-done(((bf16[1,256,256]{2,1,0:T(8,128)(2,1)}), bf16[1,2048,256]{2,1,0:T(8,128)(2,1)}) %all-gather.55.cloned.1.call-update) | async-done | bytes 1048592 | tf_op jit(solution)/shard_map/all_gather | solution.py:10
  346.7 4.8 convolution_convert_fusion.3
  351.6 36.3 %all-gather.53.cloned.1.call-done = bf16[1,2048,256]{2,1,0:T(8,128)(2,1)} async-done(((bf16[1,256,256]{2,1,0:T(8,128)(2,1)}), bf16[1,2048,256]{2,1,0:T(8,128)(2,1)}) %all-gather.53.cloned.1.call-update) | async-done | bytes 1048592 | tf_op jit(solution)/shard_map/all_gather | solution.py:10
  387.9 4.8 convolution_convert_fusion.4
  392.7 36.2 %all-gather.51.cloned.1.call-done = bf16[1,2048,256]{2,1,0:T(8,128)(2,1)} async-done(((bf16[1,256,256]{2,1,0:T(8,128)(2,1)}), bf16[1,2048,256]{2,1,0:T(8,128)(2,1)}) %all-gather.51.cloned.1.call-update) | async-done | bytes 1048592 | tf_op jit(solution)/shard_map/all_gather | solution.py:10
  428.9 4.9 convolution_convert_fusion.5
  434.0 2.5 collective-permute-start.1
  436.5 1.4 collective-permute-done.1
  437.9 1.5 fusion.20
  439.4 30.6 %all-gather.57.cloned.1.call-done = bf16[1,1024,512]{2,1,0:T(8,128)(2,1)} async-done(((bf16[1,128,512]{2,1,0:T(8,128)(2,1)}), bf16[1,1024,512]{2,1,0:T(8,128)(2,1)}) %all-gather.57.cloned.1.call-update) | async-done | bytes 1048592 | tf_op jit(solution)/shard_map/all_gather | solution.py:10
  470.0 29.1 %all-gather.37.cloned.1.call-done = bf16[6,256,1024]{2,1,0:T(8,128)(2,1)} async-done(((bf16[6,256,256]{2,1,0:T(8,128)(2,1)}), bf16[6,256,1024]{2,1,0:T(8,128)(2,1)}) %all-gather.37.cloned.1.call-update) | async-done | bytes 3145744 | tf_op jit(solution)/shard_map/all_gather | solution.py:90
  499.1 5.1 convolution_convert_fusion.9
  506.8 43.9 %all-gather.39.cloned.1.call-done = bf16[6,256,2048]{2,1,0:T(8,128)(2,1)} async-done(((bf16[6,256,512]{2,1,0:T(8,128)(2,1)}), bf16[6,256,2048]{2,1,0:T(8,128)(2,1)}) %all-gather.39.cloned.1.call-update) | async-done | bytes 6291472 | tf_op jit(solution)/shard_map/all_gather | solution.py:70
  550.8 4.2 fusion.6
  555.4 4.2 fusion.8
  559.5 33.5 %all-gather.63.cloned.1.call-done = bf16[1,2048,256]{2,1,0:T(8,128)(2,1)} async-done(((bf16[1,256,256]{2,1,0:T(8,128)(2,1)}), bf16[1,2048,256]{2,1,0:T(8,128)(2,1)}) %all-gather.63.cloned.1.call-update) | async-done | bytes 1048592 | tf_op jit(solution)/shard_map/all_gather | solution.py:10
  593.0 4.8 convolution_convert_fusion
  597.9 36.2 %all-gather.61.cloned.1.call-done = bf16[1,2048,256]{2,1,0:T(8,128)(2,1)} async-done(((bf16[1,256,256]{2,1,0:T(8,128)(2,1)}), bf16[1,2048,256]{2,1,0:T(8,128)(2,1)}) %all-gather.61.cloned.1.call-update) | async-done | bytes 1048592 | tf_op jit(solution)/shard_map/all_gather | solution.py:10
  634.0 4.8 convolution_convert_fusion.1
  638.9 36.2 %all-gather.59.cloned.1.call-done = bf16[1,2048,256]{2,1,0:T(8,128)(2,1)} async-done(((bf16[1,256,256]{2,1,0:T(8,128)(2,1)}), bf16[1,2048,256]{2,1,0:T(8,128)(2,1)}) %all-gather.59.cloned.1.call-update) | async-done | bytes 1048592 | tf_op jit(solution)/shard_map/all_gather | solution.py:10
  675.0 4.9 convolution_convert_fusion.2
  680.1 2.5 collective-permute-start.2
  682.6 1.4 collective-permute-done.2
  684.0 1.5 fusion.14
  685.5 30.5 %all-gather.65.cloned.1.call-done = bf16[1,1024,512]{2,1,0:T(8,128)(2,1)} async-done(((bf16[1,128,512]{2,1,0:T(8,128)(2,1)}), bf16[1,1024,512]{2,1,0:T(8,128)(2,1)}) %all-gather.65.cloned.1.call-update) | async-done | bytes 1048592 | tf_op jit(solution)/shard_map/all_gather | solution.py:10
  716.0 29.1 %all-gather.41.cloned.1.call-done = bf16[6,256,1024]{2,1,0:T(8,128)(2,1)} async-done(((bf16[6,256,256]{2,1,0:T(8,128)(2,1)}), bf16[6,256,1024]{2,1,0:T(8,128)(2,1)}) %all-gather.41.cloned.1.call-update) | async-done | bytes 3145744 | tf_op jit(solution)/shard_map/all_gather | solution.py:90
  745.1 5.6 fusion.30
  (66 shorter events, 9.3 us)
Async XLA Ops:
  6.5 1.0 copy-start.3
  6.5 1.8 copy-start.4
  6.5 2.7 copy-start.5
  6.5 51.5 %all-gather.31.cloned.1.call-start = ((), (), s32[]{:S(2)}) async-start(), calls=%async_computation | async-start | bytes 7864320 | tf_op jit(solution)/shard_map/all_gather | solution.py:70
  7.3 2.8 copy-start.6
  7.3 93.2 %all-gather.47.cloned.1.call-start = ((), (), s32[]{:S(2)}) async-start(), calls=%async_computation.8 | async-start | bytes 1179648 | tf_op jit(solution)/shard_map/all_gather | solution.py:10
  8.3 2.6 copy-start.7
  8.3 133.3 %all-gather.45.cloned.1.call-start = ((), (), s32[]{:S(2)}) async-start(), calls=%async_computation.7 | async-start | bytes 1179648 | tf_op jit(solution)/shard_map/all_gather | solution.py:10
  9.1 173.5 %all-gather.43.cloned.1.call-start = ((), (), s32[]{:S(2)}) async-start(), calls=%async_computation.6 | async-start | bytes 1179648 | tf_op jit(solution)/shard_map/all_gather | solution.py:10
  10.0 213.6 %all-gather.49.cloned.1.call-start = ((), (), s32[]{:S(2)}) async-start(), calls=%async_computation.9 | async-start | bytes 1179648 | tf_op jit(solution)/shard_map/all_gather | solution.py:10
  10.8 241.8 %all-gather.33.cloned.1.call-start = ((), (), s32[]{:S(2)}) async-start(), calls=%async_computation.1 | async-start | bytes 3932160 | tf_op jit(solution)/shard_map/all_gather | solution.py:90
  58.0 4.6 copy-start
  187.4 2.7 copy-start.8
  187.7 3.9 collective-permute-start
  193.0 111.3 %all-gather.35.cloned.1.call-start = ((), (), s32[]{:S(2)}) async-start(), calls=%async_computation.2 | async-start | bytes 7864320 | tf_op jit(solution)/shard_map/all_gather | solution.py:70
  257.8 88.9 %all-gather.55.cloned.1.call-start = ((), (), s32[]{:S(2)}) async-start(), calls=%async_computation.12 | async-start | bytes 1179648 | tf_op jit(solution)/shard_map/all_gather | solution.py:10
  258.5 129.3 %all-gather.53.cloned.1.call-start = ((), (), s32[]{:S(2)}) async-start(), calls=%async_computation.11 | async-start | bytes 1179648 | tf_op jit(solution)/shard_map/all_gather | solution.py:10
  259.3 169.6 %all-gather.51.cloned.1.call-start = ((), (), s32[]{:S(2)}) async-start(), calls=%async_computation.10 | async-start | bytes 1179648 | tf_op jit(solution)/shard_map/all_gather | solution.py:10
  259.9 210.2 %all-gather.57.cloned.1.call-start = ((), (), s32[]{:S(2)}) async-start(), calls=%async_computation.13 | async-start | bytes 1179648 | tf_op jit(solution)/shard_map/all_gather | solution.py:10
  260.6 238.5 %all-gather.37.cloned.1.call-start = ((), (), s32[]{:S(2)}) async-start(), calls=%async_computation.3 | async-start | bytes 3932160 | tf_op jit(solution)/shard_map/all_gather | solution.py:90
  304.3 4.6 copy-start.2
  434.0 3.9 collective-permute-start.1
  439.4 111.4 %all-gather.39.cloned.1.call-start = ((), (), s32[]{:S(2)}) async-start(), calls=%async_computation.4 | async-start | bytes 7864320 | tf_op jit(solution)/shard_map/all_gather | solution.py:70
  504.2 88.8 %all-gather.63.cloned.1.call-start = ((), (), s32[]{:S(2)}) async-start(), calls=%async_computation.16 | async-start | bytes 1179648 | tf_op jit(solution)/shard_map/all_gather | solution.py:10
  504.8 129.2 %all-gather.61.cloned.1.call-start = ((), (), s32[]{:S(2)}) async-start(), calls=%async_computation.15 | async-start | bytes 1179648 | tf_op jit(solution)/shard_map/all_gather | solution.py:10
  505.4 169.6 %all-gather.59.cloned.1.call-start = ((), (), s32[]{:S(2)}) async-start(), calls=%async_computation.14 | async-start | bytes 1179648 | tf_op jit(solution)/shard_map/all_gather | solution.py:10
  506.0 210.1 %all-gather.65.cloned.1.call-start = ((), (), s32[]{:S(2)}) async-start(), calls=%async_computation.17 | async-start | bytes 1179648 | tf_op jit(solution)/shard_map/all_gather | solution.py:10
  506.6 238.5 %all-gather.41.cloned.1.call-start = ((), (), s32[]{:S(2)}) async-start(), calls=%async_computation.5 | async-start | bytes 3932160 | tf_op jit(solution)/shard_map/all_gather | solution.py:90
  550.8 4.6 copy-start.1
  680.1 3.9 collective-permute-start.2
Sparse Core Ops, SparseCore 0:
  8.9 49.0 all-gather.30
  60.1 40.2 all-gather.46
  102.6 38.9 all-gather.44
  143.6 38.9 all-gather.42
  184.6 38.9 all-gather.48
  225.0 27.6 all-gather.32
  257.9 46.3 all-gather.34
  306.4 40.2 all-gather.54
  348.9 38.9 all-gather.52
  389.9 38.9 all-gather.50
  431.0 38.9 all-gather.56
  471.5 27.6 all-gather.36
  504.4 46.3 all-gather.38
  552.7 40.2 all-gather.62
  595.0 38.9 all-gather.60
  636.0 38.9 all-gather.58
  677.0 38.9 all-gather.64
  717.4 27.6 all-gather.40
where the time goes:
time: 758 us
  waiting for transfers between devices  641 us (85%)
  matrix products  59.6 us (8%)
  other arithmetic  30.2 us (4%)
  between operations  13.9 us (2%)
  starting transfers between devices  8.51 us (1%)
    all_gather x12, waiting for transfers between devices, taken_in(): lax.all_gather(part, axis, axis=dim, tiled=True)  410 us
    all_gather x3, waiting for transfers between devices, local(): whole = lax.all_gather(current, 'tp', axis=2, tiled=True)  134 us
    all_gather x3, waiting for transfers between devices, local(): full_mix = lax.all_gather(mixer, 'tp', axis=2, tiled=True)  87.2 us
    dot_general x9, matrix products, add_rows(): jnp.dot(columns, piece, preferred_element_type=jnp.float32)  43.7 us
    dot_general x3, matrix products, add_rows(): return total + jnp.dot(columns, piece, preferred_element_type=jnp.float32)  15.9 us
  transfers between devices with their start and end apart: 21, of which 21 were waited for; matrix products, arithmetic and copies ran while one was open for 10% of the time, Pallas kernels for 0%

commit v1 on v0

--- a/solution.py
+++ b/solution.py
@@ -87,7 +87,14 @@
         conved = convolve(extended, conv_taps[layer])
         mixer = (kept.astype(jnp.float32) * conved).astype(jnp.bfloat16)
         out_rows = mixer.shape[1]
-        full_mix = lax.all_gather(mixer, "tp", axis=2, tiled=True)
+        ring = [mixer]
+        for hop in range(3):
+            ring.append(lax.ppermute(ring[-1], "tp", [(dev, (dev + 1) % 4) for dev in range(4)]))
+        full_mix = jnp.roll(
+            jnp.concatenate(ring[::-1], axis=2),
+            (lax.axis_index("tp") + 1) * ring[0].shape[2],
+            axis=2,
+        )
         flat_mix = full_mix.reshape(sequences * out_rows, full_mix.shape[2])
         projected = project_output(flat_mix, weight_output[layer])
         result = projected.reshape(sequences, out_rows, projected.shape[1])

time: 758 us -> 705 us (0.930)
  waiting for transfers between devices: 641 us -> 583 us
    all_gather x3 -> x0, waiting for transfers between devices: 87.2 us -> none  [local(): full_mix = lax.all_gather(mixer, 'tp', axis=2, tiled=True)]
    ppermute x0 -> x9, waiting for transfers between devices: none -> 67.5 us  [local(): lax.ppermute(ring[-1], 'tp', [(dev, (dev + 1) % 4) for dev in range(4)])]
    all_gather x12, waiting for transfers between devices: 410 us -> 377 us  [taken_in(): lax.all_gather(part, axis, axis=dim, tiled=True)]
  transfers between devices with their start and end apart: 21 -> 27, of which waited for: 21 -> 24; matrix products, arithmetic and copies ran while one was open for 10% -> 9% of each run, Pallas kernels for 0% -> 0%
where the time goes in v1:
time: 705 us
  waiting for transfers between devices  583 us (83%)
  matrix products  63.9 us (9%)
  other arithmetic  27.6 us (4%)
  between operations  13.5 us (2%)
  starting transfers between devices  8.59 us (1%)
  local copies, waits for them, and re-layouts  8.12 us (1%)
    all_gather x12, waiting for transfers between devices, taken_in(): lax.all_gather(part, axis, axis=dim, tiled=True)  377 us
    all_gather x3, waiting for transfers between devices, local(): whole = lax.all_gather(current, 'tp', axis=2, tiled=True)  130 us
    ppermute x9, waiting for transfers between devices, local(): lax.ppermute(ring[-1], 'tp', [(dev, (dev + 1) % 4) for dev in range(4)])  67.5 us
    dot_general x9, matrix products, add_rows(): jnp.dot(columns, piece, preferred_element_type=jnp.float32)  43.6 us
    dot_general x3, matrix products, add_rows(): return total + jnp.dot(columns, piece, preferred_element_type=jnp.float32)  20.3 us
  transfers between devices with their start and end apart: 27, of which 24 were waited for; matrix products, arithmetic and copies ran while one was open for 9% of the time, Pallas kernels for 0%

profile of v1, /device:TPU:0, one launch (start us, length us, event | category | flops | bytes accessed | tf_op | source)
XLA Modules:
  0.0 704.9 jit_solution(14110616902194250112)
XLA Ops:
  7.3 1.8 fusion.82
  9.1 1.8 fusion.83
  11.0 1.8 fusion.84
  13.8 44.2 %all-gather.28.cloned.1.call-done = bf16[6,256,2048]{2,1,0:T(8,128)(2,1)} async-done(((bf16[6,256,512]{2,1,0:T(8,128)(2,1)}), bf16[6,256,2048]{2,1,0:T(8,128)(2,1)}) %all-gather.28.cloned.1.call-update) | async-done | bytes 6291472 | tf_op jit(solution)/shard_map/all_gather | solution.py:70
  58.0 4.2 fusion
  62.6 4.2 fusion.2
  66.8 33.7 %all-gather.38.cloned.1.call-done = bf16[1,2048,256]{2,1,0:T(8,128)(2,1)} async-done(((bf16[1,256,256]{2,1,0:T(8,128)(2,1)}), bf16[1,2048,256]{2,1,0:T(8,128)(2,1)}) %all-gather.38.cloned.1.call-update) | async-done | bytes 1048592 | tf_op jit(solution)/shard_map/all_gather | solution.py:10
  100.4 4.8 convolution_convert_fusion.6
  105.3 36.3 %all-gather.36.cloned.1.call-done = bf16[1,2048,256]{2,1,0:T(8,128)(2,1)} async-done(((bf16[1,256,256]{2,1,0:T(8,128)(2,1)}), bf16[1,2048,256]{2,1,0:T(8,128)(2,1)}) %all-gather.36.cloned.1.call-update) | async-done | bytes 1048592 | tf_op jit(solution)/shard_map/all_gather | solution.py:10
  141.6 4.9 convolution_convert_fusion.7
  146.5 36.1 %all-gather.34.cloned.1.call-done = bf16[1,2048,256]{2,1,0:T(8,128)(2,1)} async-done(((bf16[1,256,256]{2,1,0:T(8,128)(2,1)}), bf16[1,2048,256]{2,1,0:T(8,128)(2,1)}) %all-gather.34.cloned.1.call-update) | async-done | bytes 1048592 | tf_op jit(solution)/shard_map/all_gather | solution.py:10
  182.6 4.8 convolution_convert_fusion.8
  187.6 2.5 collective-permute-start
  190.2 1.4 collective-permute-done
  193.0 10.6 %collective-permute-done.1 = bf16[6,256,256]{2,1,0:T(8,128)(2,1)S(1)} collective-permute-done((bf16[6,256,256]{2,1,0:T(8,128)(2,1)S(1)}, bf16[6,256,256]{2,1,0:T(8,128)(2,1)S(1)}, u32[]{:S(2)}, u32[]{:S(2)}) %collective-permute-start.1) | collective-permute-done | bytes 786464 | tf_op jit(solution)/shard_map/ppermute | solution.py:92
  203.6 11.4 %collective-permute-done.2 = bf16[6,256,256]{2,1,0:T(8,128)(2,1)S(1)} collective-permute-done((bf16[6,256,256]{2,1,0:T(8,128)(2,1)S(1)}, bf16[6,256,256]{2,1,0:T(8,128)(2,1)S(1)}, u32[]{:S(2)}, u32[]{:S(2)}) %collective-permute-start.2) | collective-permute-done | bytes 786464 | tf_op jit(solution)/shard_map/ppermute | solution.py:92
  215.0 20.0 %all-gather.40.cloned.1.call-done = bf16[1,1024,512]{2,1,0:T(8,128)(2,1)} async-done(((bf16[1,128,512]{2,1,0:T(8,128)(2,1)}), bf16[1,1024,512]{2,1,0:T(8,128)(2,1)}) %all-gather.40.cloned.1.call-update) | async-done | bytes 1048592 | tf_op jit(solution)/shard_map/all_gather | solution.py:10
  235.0 6.8 fusion.39
  244.3 42.8 %all-gather.30.cloned.1.call-done = bf16[6,256,2048]{2,1,0:T(8,128)(2,1)} async-done(((bf16[6,256,512]{2,1,0:T(8,128)(2,1)}), bf16[6,256,2048]{2,1,0:T(8,128)(2,1)}) %all-gather.30.cloned.1.call-update) | async-done | bytes 6291472 | tf_op jit(solution)/shard_map/all_gather | solution.py:70
  287.0 4.2 fusion.3
  291.6 4.2 fusion.5
  295.8 33.7 %all-gather.46.cloned.1.call-done = bf16[1,2048,256]{2,1,0:T(8,128)(2,1)} async-done(((bf16[1,256,256]{2,1,0:T(8,128)(2,1)}), bf16[1,2048,256]{2,1,0:T(8,128)(2,1)}) %all-gather.46.cloned.1.call-update) | async-done | bytes 1048592 | tf_op jit(solution)/shard_map/all_gather | solution.py:10
  329.5 4.8 convolution_convert_fusion.3
  334.3 36.3 %all-gather.44.cloned.1.call-done = bf16[1,2048,256]{2,1,0:T(8,128)(2,1)} async-done(((bf16[1,256,256]{2,1,0:T(8,128)(2,1)}), bf16[1,2048,256]{2,1,0:T(8,128)(2,1)}) %all-gather.44.cloned.1.call-update) | async-done | bytes 1048592 | tf_op jit(solution)/shard_map/all_gather | solution.py:10
  370.6 4.9 convolution_convert_fusion.4
  375.5 36.3 %all-gather.42.cloned.1.call-done = bf16[1,2048,256]{2,1,0:T(8,128)(2,1)} async-done(((bf16[1,256,256]{2,1,0:T(8,128)(2,1)}), bf16[1,2048,256]{2,1,0:T(8,128)(2,1)}) %all-gather.42.cloned.1.call-update) | async-done | bytes 1048592 | tf_op jit(solution)/shard_map/all_gather | solution.py:10
  411.8 4.8 convolution_convert_fusion.5
  416.8 2.5 collective-permute-start.4
  419.3 1.4 collective-permute-done.4
  421.4 11.3 %collective-permute-done.5 = bf16[6,256,256]{2,1,0:T(8,128)(2,1)S(1)} collective-permute-done((bf16[6,256,256]{2,1,0:T(8,128)(2,1)S(1)}, bf16[6,256,256]{2,1,0:T(8,128)(2,1)S(1)}, u32[]{:S(2)}, u32[]{:S(2)}) %collective-permute-start.5) | collective-permute-done | bytes 786464 | tf_op jit(solution)/shard_map/ppermute | solution.py:92
  432.8 11.4 %collective-permute-done.6 = bf16[6,256,256]{2,1,0:T(8,128)(2,1)S(1)} collective-permute-done((bf16[6,256,256]{2,1,0:T(8,128)(2,1)S(1)}, bf16[6,256,256]{2,1,0:T(8,128)(2,1)S(1)}, u32[]{:S(2)}, u32[]{:S(2)}) %collective-permute-start.6) | collective-permute-done | bytes 786464 | tf_op jit(solution)/shard_map/ppermute | solution.py:92
  444.2 19.3 %all-gather.48.cloned.1.call-done = bf16[1,1024,512]{2,1,0:T(8,128)(2,1)} async-done(((bf16[1,128,512]{2,1,0:T(8,128)(2,1)}), bf16[1,1024,512]{2,1,0:T(8,128)(2,1)}) %all-gather.48.cloned.1.call-update) | async-done | bytes 1048592 | tf_op jit(solution)/shard_map/all_gather | solution.py:10
  463.5 6.8 fusion.36
  472.4 43.0 %all-gather.32.cloned.1.call-done = bf16[6,256,2048]{2,1,0:T(8,128)(2,1)} async-done(((bf16[6,256,512]{2,1,0:T(8,128)(2,1)}), bf16[6,256,2048]{2,1,0:T(8,128)(2,1)}) %all-gather.32.cloned.1.call-update) | async-done | bytes 6291472 | tf_op jit(solution)/shard_map/all_gather | solution.py:70
  515.5 4.2 fusion.6
  520.1 4.2 fusion.8
  524.2 33.5 %all-gather.54.cloned.1.call-done = bf16[1,2048,256]{2,1,0:T(8,128)(2,1)} async-done(((bf16[1,256,256]{2,1,0:T(8,128)(2,1)}), bf16[1,2048,256]{2,1,0:T(8,128)(2,1)}) %all-gather.54.cloned.1.call-update) | async-done | bytes 1048592 | tf_op jit(solution)/shard_map/all_gather | solution.py:10
  557.8 4.8 convolution_convert_fusion
  562.6 36.3 %all-gather.52.cloned.1.call-done = bf16[1,2048,256]{2,1,0:T(8,128)(2,1)} async-done(((bf16[1,256,256]{2,1,0:T(8,128)(2,1)}), bf16[1,2048,256]{2,1,0:T(8,128)(2,1)}) %all-gather.52.cloned.1.call-update) | async-done | bytes 1048592 | tf_op jit(solution)/shard_map/all_gather | solution.py:10
  598.9 4.9 convolution_convert_fusion.1
  603.8 36.1 %all-gather.50.cloned.1.call-done = bf16[1,2048,256]{2,1,0:T(8,128)(2,1)} async-done(((bf16[1,256,256]{2,1,0:T(8,128)(2,1)}), bf16[1,2048,256]{2,1,0:T(8,128)(2,1)}) %all-gather.50.cloned.1.call-update) | async-done | bytes 1048592 | tf_op jit(solution)/shard_map/all_gather | solution.py:10
  639.9 4.8 convolution_convert_fusion.2
  644.9 2.5 collective-permute-start.8
  647.4 1.4 collective-permute-done.8
  649.5 11.4 %collective-permute-done.9 = bf16[6,256,256]{2,1,0:T(8,128)(2,1)S(1)} collective-permute-done((bf16[6,256,256]{2,1,0:T(8,128)(2,1)S(1)}, bf16[6,256,256]{2,1,0:T(8,128)(2,1)S(1)}, u32[]{:S(2)}, u32[]{:S(2)}) %collective-permute-start.9) | collective-permute-done | bytes 786464 | tf_op jit(solution)/shard_map/ppermute | solution.py:92
  660.9 11.4 %collective-permute-done.10 = bf16[6,256,256]{2,1,0:T(8,128)(2,1)S(1)} collective-permute-done((bf16[6,256,256]{2,1,0:T(8,128)(2,1)S(1)}, bf16[6,256,256]{2,1,0:T(8,128)(2,1)S(1)}, u32[]{:S(2)}, u32[]{:S(2)}) %collective-permute-start.10) | collective-permute-done | bytes 786464 | tf_op jit(solution)/shard_map/ppermute | solution.py:92
  672.3 19.3 %all-gather.56.cloned.1.call-done = bf16[1,1024,512]{2,1,0:T(8,128)(2,1)} async-done(((bf16[1,128,512]{2,1,0:T(8,128)(2,1)}), bf16[1,1024,512]{2,1,0:T(8,128)(2,1)}) %all-gather.56.cloned.1.call-update) | async-done | bytes 1048592 | tf_op jit(solution)/shard_map/all_gather | solution.py:10
  691.6 6.7 fusion.34
  (67 shorter events, 10.9 us)
Async XLA Ops:
  6.5 51.5 %all-gather.28.cloned.1.call-start = ((), (), s32[]{:S(2)}) async-start(), calls=%async_computation | async-start | bytes 7864320 | tf_op jit(solution)/shard_map/all_gather | solution.py:70
  7.3 93.2 %all-gather.38.cloned.1.call-start = ((), (), s32[]{:S(2)}) async-start(), calls=%async_computation.5 | async-start | bytes 1179648 | tf_op jit(solution)/shard_map/all_gather | solution.py:10
  9.1 132.5 %all-gather.36.cloned.1.call-start = ((), (), s32[]{:S(2)}) async-start(), calls=%async_computation.4 | async-start | bytes 1179648 | tf_op jit(solution)/shard_map/all_gather | solution.py:10
  11.0 171.6 %all-gather.34.cloned.1.call-start = ((), (), s32[]{:S(2)}) async-start(), calls=%async_computation.3 | async-start | bytes 1179648 | tf_op jit(solution)/shard_map/all_gather | solution.py:10
  12.8 222.2 %all-gather.40.cloned.1.call-start = ((), (), s32[]{:S(2)}) async-start(), calls=%async_computation.6 | async-start | bytes 1179648 | tf_op jit(solution)/shard_map/all_gather | solution.py:10
  58.0 4.6 copy-start
  146.5 43.7 %copy-start.4 = (bf16[3,3,256]{2,1,0:T(4,128)(2,1)S(1)}, bf16[3,3,256]{2,1,0:T(4,128)(2,1)}, u32[]{:S(2)}) copy-start(bf16[3,3,256]{2,1,0:T(4,128)(2,1)} %param.14) | copy-start | bytes 13828
  187.4 4.8 copy-start.3
  187.6 3.9 collective-permute-start
  192.1 11.5 %collective-permute-start.1 = (bf16[6,256,256]{2,1,0:T(8,128)(2,1)S(1)}, bf16[6,256,256]{2,1,0:T(8,128)(2,1)S(1)}, u32[]{:S(2)}, u32[]{:S(2)}) collective-permute-start(bf16[6,256,256]{2,1,0:T(8,128)(2,1)S(1)} %fusion.59), channel_id=1, source_target_pairs={{0,1},{1,2},{2,3},{3,0},{4,5},{5,6},{6,7},{7,4},{8,9},{9,10},{10,1... | collective-permute-start | bytes 2359304 | tf_op jit(solution)/shard_map/ppermute | solution.py:92
  193.0 94.1 %all-gather.30.cloned.1.call-start = ((), (), s32[]{:S(2)}) async-start(), calls=%async_computation.1 | async-start | bytes 7864320 | tf_op jit(solution)/shard_map/all_gather | solution.py:70
  203.6 11.4 %collective-permute-start.2 = (bf16[6,256,256]{2,1,0:T(8,128)(2,1)S(1)}, bf16[6,256,256]{2,1,0:T(8,128)(2,1)S(1)}, u32[]{:S(2)}, u32[]{:S(2)}) collective-permute-start(bf16[6,256,256]{2,1,0:T(8,128)(2,1)S(1)} %collective-permute-done.1), channel_id=1, source_target_pairs={{0,1},{1,2},{2,3},{3,0},{4,5},{5,6},{6,7},{7,4},{8,9},{9,10},{10,1... | collective-permute-start | bytes 2359304 | tf_op jit(solution)/shard_map/ppermute | solution.py:92
  215.0 20.0 %collective-permute-start.3 = (bf16[6,256,256]{2,1,0:T(8,128)(2,1)S(1)}, bf16[6,256,256]{2,1,0:T(8,128)(2,1)S(1)}, u32[]{:S(2)}, u32[]{:S(2)}) collective-permute-start(bf16[6,256,256]{2,1,0:T(8,128)(2,1)S(1)} %collective-permute-done.2), channel_id=1, source_target_pairs={{0,1},{1,2},{2,3},{3,0},{4,5},{5,6},{6,7},{7,4},{8,9},{9,10},{10,1... | collective-permute-start | bytes 2359304 | tf_op jit(solution)/shard_map/ppermute | solution.py:92
  241.8 87.7 %all-gather.46.cloned.1.call-start = ((), (), s32[]{:S(2)}) async-start(), calls=%async_computation.9 | async-start | bytes 1179648 | tf_op jit(solution)/shard_map/all_gather | solution.py:10
  242.6 128.1 %all-gather.44.cloned.1.call-start = ((), (), s32[]{:S(2)}) async-start(), calls=%async_computation.8 | async-start | bytes 1179648 | tf_op jit(solution)/shard_map/all_gather | solution.py:10
  243.3 168.5 %all-gather.42.cloned.1.call-start = ((), (), s32[]{:S(2)}) async-start(), calls=%async_computation.7 | async-start | bytes 1179648 | tf_op jit(solution)/shard_map/all_gather | solution.py:10
  244.0 219.4 %all-gather.48.cloned.1.call-start = ((), (), s32[]{:S(2)}) async-start(), calls=%async_computation.10 | async-start | bytes 1179648 | tf_op jit(solution)/shard_map/all_gather | solution.py:10
  287.0 4.6 copy-start.2
  416.8 3.9 collective-permute-start.4
  421.3 11.5 %collective-permute-start.5 = (bf16[6,256,256]{2,1,0:T(8,128)(2,1)S(1)}, bf16[6,256,256]{2,1,0:T(8,128)(2,1)S(1)}, u32[]{:S(2)}, u32[]{:S(2)}) collective-permute-start(bf16[6,256,256]{2,1,0:T(8,128)(2,1)S(1)} %fusion.53), channel_id=1, source_target_pairs={{0,1},{1,2},{2,3},{3,0},{4,5},{5,6},{6,7},{7,4},{8,9},{9,10},{10,1... | collective-permute-start | bytes 2359304 | tf_op jit(solution)/shard_map/ppermute | solution.py:92
  421.4 94.1 %all-gather.32.cloned.1.call-start = ((), (), s32[]{:S(2)}) async-start(), calls=%async_computation.2 | async-start | bytes 7864320 | tf_op jit(solution)/shard_map/all_gather | solution.py:70
  432.8 11.4 %collective-permute-start.6 = (bf16[6,256,256]{2,1,0:T(8,128)(2,1)S(1)}, bf16[6,256,256]{2,1,0:T(8,128)(2,1)S(1)}, u32[]{:S(2)}, u32[]{:S(2)}) collective-permute-start(bf16[6,256,256]{2,1,0:T(8,128)(2,1)S(1)} %collective-permute-done.5), channel_id=1, source_target_pairs={{0,1},{1,2},{2,3},{3,0},{4,5},{5,6},{6,7},{7,4},{8,9},{9,10},{10,1... | collective-permute-start | bytes 2359304 | tf_op jit(solution)/shard_map/ppermute | solution.py:92
  444.2 19.3 %collective-permute-start.7 = (bf16[6,256,256]{2,1,0:T(8,128)(2,1)S(1)}, bf16[6,256,256]{2,1,0:T(8,128)(2,1)S(1)}, u32[]{:S(2)}, u32[]{:S(2)}) collective-permute-start(bf16[6,256,256]{2,1,0:T(8,128)(2,1)S(1)} %collective-permute-done.6), channel_id=1, source_target_pairs={{0,1},{1,2},{2,3},{3,0},{4,5},{5,6},{6,7},{7,4},{8,9},{9,10},{10,1... | collective-permute-start | bytes 2359304 | tf_op jit(solution)/shard_map/ppermute | solution.py:92
  470.3 87.5 %all-gather.54.cloned.1.call-start = ((), (), s32[]{:S(2)}) async-start(), calls=%async_computation.13 | async-start | bytes 1179648 | tf_op jit(solution)/shard_map/all_gather | solution.py:10
  470.8 128.1 %all-gather.52.cloned.1.call-start = ((), (), s32[]{:S(2)}) async-start(), calls=%async_computation.12 | async-start | bytes 1179648 | tf_op jit(solution)/shard_map/all_gather | solution.py:10
  471.6 168.3 %all-gather.50.cloned.1.call-start = ((), (), s32[]{:S(2)}) async-start(), calls=%async_computation.11 | async-start | bytes 1179648 | tf_op jit(solution)/shard_map/all_gather | solution.py:10
  472.2 219.4 %all-gather.56.cloned.1.call-start = ((), (), s32[]{:S(2)}) async-start(), calls=%async_computation.14 | async-start | bytes 1179648 | tf_op jit(solution)/shard_map/all_gather | solution.py:10
  515.5 4.6 copy-start.1
  644.9 3.9 collective-permute-start.8
  649.4 11.5 %collective-permute-start.9 = (bf16[6,256,256]{2,1,0:T(8,128)(2,1)S(1)}, bf16[6,256,256]{2,1,0:T(8,128)(2,1)S(1)}, u32[]{:S(2)}, u32[]{:S(2)}) collective-permute-start(bf16[6,256,256]{2,1,0:T(8,128)(2,1)S(1)} %fusion.47), channel_id=1, source_target_pairs={{0,1},{1,2},{2,3},{3,0},{4,5},{5,6},{6,7},{7,4},{8,9},{9,10},{10,1... | collective-permute-start | bytes 2359304 | tf_op jit(solution)/shard_map/ppermute | solution.py:92
  660.9 11.4 %collective-permute-start.10 = (bf16[6,256,256]{2,1,0:T(8,128)(2,1)S(1)}, bf16[6,256,256]{2,1,0:T(8,128)(2,1)S(1)}, u32[]{:S(2)}, u32[]{:S(2)}) collective-permute-start(bf16[6,256,256]{2,1,0:T(8,128)(2,1)S(1)} %collective-permute-done.9), channel_id=1, source_target_pairs={{0,1},{1,2},{2,3},{3,0},{4,5},{5,6},{6,7},{7,4},{8,9},{9,10},{10,1... | collective-permute-start | bytes 2359304 | tf_op jit(solution)/shard_map/ppermute | solution.py:92
  672.3 19.3 %collective-permute-start.11 = (bf16[6,256,256]{2,1,0:T(8,128)(2,1)S(1)}, bf16[6,256,256]{2,1,0:T(8,128)(2,1)S(1)}, u32[]{:S(2)}, u32[]{:S(2)}) collective-permute-start(bf16[6,256,256]{2,1,0:T(8,128)(2,1)S(1)} %collective-permute-done.10), channel_id=1, source_target_pairs={{0,1},{1,2},{2,3},{3,0},{4,5},{5,6},{6,7},{7,4},{8,9},{9,10},{10,1... | collective-permute-start | bytes 2359304 | tf_op jit(solution)/shard_map/ppermute | solution.py:92
Sparse Core Ops, SparseCore 0:
  8.9 49.0 all-gather.27
  60.1 40.2 all-gather.37
  102.6 38.9 all-gather.35
  143.6 38.9 all-gather.33
  193.1 41.8 all-gather.39
  241.9 45.0 all-gather.29
  289.2 40.2 all-gather.45
  331.6 38.9 all-gather.43
  372.7 38.9 all-gather.41
  421.5 41.9 all-gather.47
  470.4 45.0 all-gather.31
  517.5 40.2 all-gather.53
  559.9 38.9 all-gather.51
  600.9 38.9 all-gather.49
  649.7 41.9 all-gather.55
